TPU v7x, 512 devices: a 8x2x16 block of a 8x8x16 slice. The times are simulated.
512 devices in a mesh: grp: 2 (over y), sp: 16 (over z), dp: 16 (over x, core).
Axes of the slice: x: 8, y: 2, z: 16, core: 2. Of those that a mesh axis runs over, the one named last changes fastest.
The devices are a block of a 8x8x16 slice.
Arguments:
- tokens: bfloat16 [32, 2560, 2048], P(('grp', 'dp'), 'sp'), parts along dimension 0, may hold values from -6 to 6
- query_weight: bfloat16 [2048, 1024], P('dp'), may hold values from -0.125 to 0.125
- key_weight: bfloat16 [2048, 256], P('dp'), may hold values from -0.125 to 0.125
- value_weight: bfloat16 [2048, 256], P('dp'), may hold values from -0.125 to 0.125
- out_weight: bfloat16 [1024, 2048], P(None, 'dp'), may hold values from -0.1875 to 0.1875
- query_gain: float32 [64], replicated, may hold values from 0.28 to 6
- key_gain: float32 [64], replicated, may hold values from 0.28 to 6
Outputs:
- mixed: bfloat16 [32, 2560, 2048], P(('grp', 'dp'), 'sp'), parts along dimension 0
There are 2 independent parts, one for each index of `grp`. A program takes and returns all parts, laid end to end along the dimension named above; an argument that names none is the same for every part. Nothing has to cross between parts.
All inputs are finite; a program needn't handle non-finite values.
Results may differ from a plain program's by a relative error of at most 0.006.
The roundings to bfloat16 on the way count: a program that leaves them out, or rounds other values in their place, can miss the bound.
Values may be sent and summed in bfloat16 or wider, within the bound.
A program may use at most 64 MiB of HBM per device.

v0:
```python
import jax
import jax.numpy as jnp
from jax import lax
from jax.sharding import PartitionSpec as P

HEADS = 16
KV_HEADS = 4
HEAD_DIM = 64
GRID_W = 64
theta_base = 10000.0
norm_eps = 1e-06


def sent_together(arrays, axis, dim, along):
    ends, at = ([], 0)
    for a in arrays[:-1]:
        at += a.shape[along]
        ends.append(at)
    both = jnp.concatenate(arrays, axis=along)
    return tuple(jnp.split(lax.all_gather(both, axis, axis=dim, tiled=True), ends, axis=along))


def rotary_tables(positions):
    quarter = HEAD_DIM // 4
    inverse = theta_base ** (-jnp.arange(quarter, dtype=jnp.float32) / quarter)
    grid_rows = (positions // GRID_W).astype(jnp.float32)
    grid_cols = (positions % GRID_W).astype(jnp.float32)
    angles = jnp.concatenate([grid_rows[:, None] * inverse, grid_cols[:, None] * inverse], axis=-1)
    return (jnp.cos(angles), jnp.sin(angles))


def norm_rotate(raw, gain, cosine, sine):
    scaled = raw * lax.rsqrt(jnp.mean(raw * raw, axis=-1, keepdims=True) + norm_eps) * gain
    half = HEAD_DIM // 2
    first_half = scaled[..., :half]
    second_half = scaled[..., half:]
    cosine = cosine[:, None, :]
    sine = sine[:, None, :]
    turned = jnp.concatenate(
        [first_half * cosine - second_half * sine, second_half * cosine + first_half * sine],
        axis=-1,
    )
    return turned.astype(jnp.bfloat16)


def attend_block(queries, keys, values):
    scale = HEAD_DIM ** (-0.5)
    scores = jnp.einsum("qkgd,skd->kgqs", queries, keys, preferred_element_type=jnp.float32) * scale
    top = jnp.max(scores, axis=-1, keepdims=True)
    weights = jnp.exp(scores - top)
    probs = (weights / jnp.sum(weights, axis=-1, keepdims=True)).astype(jnp.bfloat16)
    result = jnp.einsum("kgqs,skd->qkgd", probs, values, preferred_element_type=jnp.float32).astype(
        jnp.bfloat16
    )
    return result.reshape(queries.shape[0], -1)


def shards(tokens, query_weight, key_weight, value_weight, out_weight, query_gain, key_gain):
    tok_rows = tokens.shape[1]
    local_rows = tokens.reshape(tok_rows, tokens.shape[2])
    seq_index = lax.axis_index("sp")
    per_kv = HEADS // KV_HEADS
    pieces = sent_together((query_weight, key_weight, value_weight), "dp", 0, 1)
    raw_q, raw_k, raw_v = tuple(
        (jnp.dot(local_rows, piece, preferred_element_type=jnp.float32) for piece in pieces)
    )
    positions = seq_index * tok_rows + jnp.arange(tok_rows, dtype=jnp.int32)
    cosine, sine = rotary_tables(positions)
    queries = norm_rotate(raw_q.reshape(tok_rows, HEADS, HEAD_DIM), query_gain, cosine, sine)
    keys = norm_rotate(raw_k.reshape(tok_rows, KV_HEADS, HEAD_DIM), key_gain, cosine, sine)
    values = raw_v.astype(jnp.bfloat16).reshape(tok_rows, KV_HEADS, HEAD_DIM)
    kv_pair = jnp.stack(
        [
            keys.reshape(tok_rows, KV_HEADS * HEAD_DIM),
            values.reshape(tok_rows, KV_HEADS * HEAD_DIM),
        ],
        axis=1,
    )
    whole_kv = lax.all_gather(kv_pair, "sp", axis=0, tiled=True)
    length = whole_kv.shape[0]
    all_k = whole_kv[:, 0].reshape(length, KV_HEADS, HEAD_DIM).transpose(1, 0, 2)[:, :, None, :]
    all_v = whole_kv[:, 1].reshape(length, KV_HEADS, HEAD_DIM).transpose(1, 0, 2)[:, :, None, :]
    grouped_q = queries.reshape(tok_rows, KV_HEADS, 1, per_kv, HEAD_DIM).transpose(1, 0, 2, 3, 4)

    def kv_head(operands):
        block_q, block_k, block_v = operands
        return attend_block(block_q, block_k, block_v)

    per_head = lax.map(kv_head, (grouped_q, all_k, all_v))
    attended = per_head.transpose(1, 0, 2).reshape(tok_rows, HEADS * HEAD_DIM)
    result = jnp.dot(
        attended,
        lax.all_gather(out_weight, "dp", axis=1, tiled=True),
        preferred_element_type=jnp.float32,
    )
    return result.astype(jnp.bfloat16).reshape(1, tok_rows, result.shape[1])


def solution(mesh):
    in_specs = (
        P(("grp", "dp"), "sp", None),
        P("dp", None),
        P("dp", None),
        P("dp", None),
        P(None, "dp"),
        P(),
        P(),
    )
    out_specs = P(("grp", "dp"), "sp", None)
    return jax.shard_map(shards, mesh=mesh, in_specs=in_specs, out_specs=out_specs, check_vma=False)
```

profile of v0, /device:TPU:65, one launch (start us, length us, event | category | flops | bytes accessed | tf_op | source)
XLA Modules:
  0.0 242.1 jit_solution(6979037957639061434)
XLA Ops:
  6.6 1.8 pad_maximum_fusion
  8.8 88.1 %all-gather.4.cloned.1.call-done = bf16[2048,1536]{1,0:T(8,128)(2,1)} async-done(((bf16[128,1536]{1,0:T(8,128)(2,1)}), bf16[2048,1536]{1,0:T(8,128)(2,1)}) %all-gather.4.cloned.1.call-update) | async-done | bytes 6291472 | tf_op jit(solution)/shard_map/all_gather | solution.py:20
  96.9 1.6 convolution_bitcast_fusion
  98.9 1.6 fusion.23
  100.5 0.7 pad_maximum_fusion.1
  101.3 0.7 all-gather.8.cloned.1.call-update
  102.2 3.0 %fusion.20 = f32[160,1024]{1,0:T(8,128)S(1)} fusion(bf16[2048,1536]{1,0:T(8,128)(2,1)} %all-gather.4.cloned.1.call-done, bf16[1,160,2048]{2,1,0:T(8,128)(2,1)S(1)} %copy-done), kind=kOutput, calls=%fused_computation.27 | convolution fusion | flops 671088640 | bytes 5505024 | tf_op jit(solution)/shard_map/dot_general | solution.py:65
  106.5 0.6 subtract_convert_fusion
  108.2 0.9 maximum_bitcast_fusion
  109.1 57.9 %all-gather.6.cloned.1.call-done = bf16[2560,2,256]{2,0,1:T(8,128)(2,1)} async-done(((bf16[160,2,256]{2,0,1:T(8,128)(2,1)}), bf16[2560,2,256]{2,0,1:T(8,128)(2,1)}) %all-gather.6.cloned.1.call-update) | async-done | bytes 2621456 | tf_op jit(solution)/shard_map/all_gather | solution.py:79
  167.0 1.9 fusion.34
  168.9 1.6 copy.14
  170.5 0.7 copy.15
  171.3 27.9 %while.10 = (s32[]{:T(128)}, bf16[4,160,256]{1,2,0:T(8,128)(2,1)}, bf16[4,2560,1,64]{1,3,2,0:T(8,128)(2,1)}, bf16[4,2560,1,64]{1,3,2,0:T(8,128)(2,1)S(1)}, bf16[4,160,1,4,64]{1,4,3,2,0:T(8,128)(2,1)}, /*index=5*/s32[]{:T(128)}) while((s32[]{:T(128)}, bf16[4,160,256]{1,2,0:T(8,128)(2,1)}, bf16[4,2560,1,64]{1,3,2,0:T(8,128)(2,1)}, ...), condition=%wide.region_5.6_spmd, body=%wide.region_2.5_spmd.sunk | while | flops 434215680 | bytes 20757060 | solution.py:89
  171.3 2.1 bitcast_reduce_fusion.2
  173.4 1.2 fusion.43
  174.7 2.9 %fusion.44 = bf16[64,4,160]{2,0,1:T(8,128)(2,1)S(1)} fusion(f32[4,160]{1,0:T(4,128)S(1)} %fusion.43, f32[4,160]{1,0:T(4,128)S(1)} %get-tuple-element.96, f32[2560,160,4]{0,1,2:T(8,128)S(1)} %get-tuple-element.95, bf16[4,2560,1,64]{1,3,2,0:T(8,128)(2,1)} %get-tuple-element.111, s32[]{:T(128)} %get-tuple-element.103), kind=kOutput, calls=%fused_computation.7.clone.1 | convolution fusion | flops 216309760 | bytes 6968832 | tf_op jit(solution)/shard_map/while/body/eval_jaxpr/kgqs,skd->qkgd/dot_general | solution.py:52
  177.6 0.7 constant_dynamic-update-slice_fusion.2
  178.2 2.1 bitcast_reduce_fusion.2
  180.4 1.2 fusion.43
  181.6 2.9 %fusion.44 = bf16[64,4,160]{2,0,1:T(8,128)(2,1)S(1)} fusion(f32[4,160]{1,0:T(4,128)S(1)} %fusion.43, f32[4,160]{1,0:T(4,128)S(1)} %get-tuple-element.96, f32[2560,160,4]{0,1,2:T(8,128)S(1)} %get-tuple-element.95, bf16[4,2560,1,64]{1,3,2,0:T(8,128)(2,1)} %get-tuple-element.111, s32[]{:T(128)} %get-tuple-element.103), kind=kOutput, calls=%fused_computation.7.clone.1 | convolution fusion | flops 216309760 | bytes 6968832 | tf_op jit(solution)/shard_map/while/body/eval_jaxpr/kgqs,skd->qkgd/dot_general | solution.py:52
  184.5 0.7 constant_dynamic-update-slice_fusion.2
  185.2 2.1 bitcast_reduce_fusion.2
  187.3 1.2 fusion.43
  188.6 2.9 %fusion.44 = bf16[64,4,160]{2,0,1:T(8,128)(2,1)S(1)} fusion(f32[4,160]{1,0:T(4,128)S(1)} %fusion.43, f32[4,160]{1,0:T(4,128)S(1)} %get-tuple-element.96, f32[2560,160,4]{0,1,2:T(8,128)S(1)} %get-tuple-element.95, bf16[4,2560,1,64]{1,3,2,0:T(8,128)(2,1)} %get-tuple-element.111, s32[]{:T(128)} %get-tuple-element.103), kind=kOutput, calls=%fused_computation.7.clone.1 | convolution fusion | flops 216309760 | bytes 6968832 | tf_op jit(solution)/shard_map/while/body/eval_jaxpr/kgqs,skd->qkgd/dot_general | solution.py:52
  191.5 0.7 constant_dynamic-update-slice_fusion.2
  192.1 2.2 bitcast_reduce_fusion.2
  194.3 1.2 fusion.43
  195.5 2.9 %fusion.44 = bf16[64,4,160]{2,0,1:T(8,128)(2,1)S(1)} fusion(f32[4,160]{1,0:T(4,128)S(1)} %fusion.43, f32[4,160]{1,0:T(4,128)S(1)} %get-tuple-element.96, f32[2560,160,4]{0,1,2:T(8,128)S(1)} %get-tuple-element.95, bf16[4,2560,1,64]{1,3,2,0:T(8,128)(2,1)} %get-tuple-element.111, s32[]{:T(128)} %get-tuple-element.103), kind=kOutput, calls=%fused_computation.7.clone.1 | convolution fusion | flops 216309760 | bytes 6968832 | tf_op jit(solution)/shard_map/while/body/eval_jaxpr/kgqs,skd->qkgd/dot_general | solution.py:52
  198.5 0.7 constant_dynamic-update-slice_fusion.2
  199.1 32.3 %all-gather.8.cloned.1.call-done = bf16[1024,2048]{1,0:T(8,128)(2,1)} async-done(((bf16[1024,128]{1,0:T(8,128)(2,1)}), bf16[1024,2048]{1,0:T(8,128)(2,1)}) %all-gather.8.cloned.1.call-update) | async-done | bytes 4194320 | tf_op jit(solution)/shard_map/all_gather | solution.py:93
  231.5 4.1 %fusion.19 = bf16[1,160,2048]{2,1,0:T(8,128)(2,1)} fusion(bf16[160,1024]{0,1:T(8,128)(2,1)} %bitcast.109, bf16[1024,2048]{1,0:T(8,128)(2,1)} %all-gather.8.cloned.1.call-done), kind=kOutput, calls=%fused_computation.22 | convolution fusion | flops 671416320 | bytes 5177344 | tf_op jit(solution)/shard_map/dot_general | solution.py:91
  (31 shorter events, 3.4 us)
Async XLA Ops:
  6.5 90.3 %copy-start = (bf16[1,160,2048]{2,1,0:T(8,128)(2,1)S(1)}, bf16[1,160,2048]{2,1,0:T(8,128)(2,1)}, u32[]{:S(2)}) copy-start(bf16[1,160,2048]{2,1,0:T(8,128)(2,1)} %param.9) | copy-start | bytes 1966084
  6.6 92.1 %copy-start.1 = (f32[64]{0:T(128)S(1)}, f32[64]{0:T(128)}, u32[]{:S(2)}) copy-start(f32[64]{0:T(128)} %param.15) | copy-start | bytes 772
  6.6 90.3 %all-gather.4.cloned.1.call-start = ((), (), s32[]{:S(2)}) async-start(), calls=%async_computation | async-start | bytes 6684672 | tf_op jit(solution)/shard_map/all_gather | solution.py:20
  8.5 158.6 %all-gather.6.cloned.1.call-start = ((), (), s32[]{:S(2)}) async-start(), calls=%async_computation.1 | async-start | bytes 2785280 | tf_op jit(solution)/shard_map/all_gather | solution.py:79
  101.2 130.2 %all-gather.8.cloned.1.call-start = ((), (), s32[]{:S(2)}) async-start(), calls=%async_computation.2 | async-start | bytes 4456448 | tf_op jit(solution)/shard_map/all_gather | solution.py:93
  105.3 0.8 copy-start.2
Sparse Core Ops, SparseCore 0:
  9.5 87.3 all-gather.3
  101.4 65.6 all-gather.5
  169.1 62.3 all-gather.7
where the time goes:
time: 243 us; the launch traced here: 242 us
  waiting for transfers between devices  179 us (74%)
  matrix products  30.5 us (13%)
  between operations  13.3 us (5%)
  other arithmetic  10.2 us (4%)
  local copies, waits for them, and re-layouts  8.79 us (4%)
    all_gather x1, waiting for transfers between devices, sent_together(): lax.all_gather(both, axis, axis=dim, tiled=True)  88.1 us
    all_gather x1, waiting for transfers between devices, shards(): whole_kv = lax.all_gather(kv_pair, 'sp', axis=0, tiled=True)  57.9 us
    all_gather x1, waiting for transfers between devices, shards(): lax.all_gather(out_weight, 'dp', axis=1, tiled=True)  32.3 us
    dot_general x4, matrix products, attend_block(): jnp.einsum('kgqs,skd->qkgd', probs, values, preferred_element_type=jnp.fl...  11.6 us
    dot_general x4, matrix products, attend_block(): jnp.einsum('qkgd,skd->kgqs', queries, keys, preferred_element_type=jnp.fl...  8.6 us
    dot_general x3, matrix products, shards(): jnp.dot(local_rows, piece, preferred_element_type=jnp.float32)  6.16 us
    reduce_sum x4, other arithmetic, attend_block(): jnp.sum(weights, axis=-1, keepdims=True)  4.88 us
  transfers between devices with their start and end apart: 3, of which 3 were waited for; matrix products, arithmetic and copies ran while one was open for 16% of the time, Pallas kernels for 0%

commit v1 on v0

--- a/solution.py
+++ b/solution.py
@@ -9,6 +9,25 @@
 GRID_W = 64
 theta_base = 10000.0
 norm_eps = 1e-06
+
+
+def task_measure(original, mesh_dim):
+    part_next = lax.axis_size(mesh_dim)
+    s_next = lax.axis_index(mesh_dim)
+    y1, lower, x_new = (part_next, s_next, original.shape[0])
+    all_rows = [(it, (it + 1) % y1) for it in range(y1)]
+    pages = [(it, (it - 1) % y1) for it in range(y1)]
+    res = jnp.zeros((*original.shape[:0], y1 * x_new, *original.shape[1:]), original.dtype)
+    res = lax.dynamic_update_slice_in_dim(res, original, lower * x_new, axis=0)
+    tall = z1 = original
+    f_next = y1 // 2
+    for m in range(1, f_next + 1):
+        tall = lax.ppermute(tall, mesh_dim, all_rows)
+        res = lax.dynamic_update_slice_in_dim(res, tall, (lower - m) % y1 * x_new, axis=0)
+        if m < y1 - f_next:
+            z1 = lax.ppermute(z1, mesh_dim, pages)
+            res = lax.dynamic_update_slice_in_dim(res, z1, (lower + m) % y1 * x_new, axis=0)
+    return res
 
 
 def sent_together(arrays, axis, dim, along):
@@ -76,7 +95,7 @@
         ],
         axis=1,
     )
-    whole_kv = lax.all_gather(kv_pair, "sp", axis=0, tiled=True)
+    whole_kv = task_measure(kv_pair, "sp")
     length = whole_kv.shape[0]
     all_k = whole_kv[:, 0].reshape(length, KV_HEADS, HEAD_DIM).transpose(1, 0, 2)[:, :, None, :]
     all_v = whole_kv[:, 1].reshape(length, KV_HEADS, HEAD_DIM).transpose(1, 0, 2)[:, :, None, :]

time: 243 us -> 277 us (1.14)
  the two profiles are of different devices: /device:TPU:65 before, /device:TPU:66 now
where the time goes in v1:
time: 277 us; the launch traced here: 276 us
  waiting for transfers between devices  93.5 us (34%)
  local copies, waits for them, and re-layouts  71.7 us (26%)
  starting transfers between devices  55.1 us (20%)
  matrix products  30.8 us (11%)
  between operations  14.4 us (5%)
  other arithmetic  10.5 us (4%)
    all_gather x1, waiting for transfers between devices, sent_together(): lax.all_gather(both, axis, axis=dim, tiled=True)  86.2 us
    ppermute x7, starting transfers between devices, task_measure(): z1 = lax.ppermute(z1, mesh_dim, pages)  37.8 us
    dynamic_update_slice x8, local copies, waits for them, and re-layouts, task_measure(): lax.dynamic_update_slice_in_dim(res, tall, (lower - m) % y1 * x_new, axis=0)  22.2 us
    dynamic_update_slice x7, local copies, waits for them, and re-layouts, task_measure(): lax.dynamic_update_slice_in_dim(res, z1, (lower + m) % y1 * x_new, axis=0)  21.4 us
    ppermute x8, starting transfers between devices, task_measure(): tall = lax.ppermute(tall, mesh_dim, all_rows)  17.2 us
    dot_general x4, matrix products, attend_block(): jnp.einsum('kgqs,skd->qkgd', probs, values, preferred_element_type=jnp.fl...  11.6 us
    dot_general x4, matrix products, attend_block(): jnp.einsum('qkgd,skd->kgqs', queries, keys, preferred_element_type=jnp.fl...  8.94 us
    ppermute x8, local copies, waits for them, and re-layouts, task_measure(): tall = lax.ppermute(tall, mesh_dim, all_rows)  8.38 us
  transfers between devices with their start and end apart: 17, of which 9 were waited for; matrix products, arithmetic and copies ran while one was open for 37% of the time, Pallas kernels for 0%

profile of v1, /device:TPU:66, one launch (start us, length us, event | category | flops | bytes accessed | tf_op | source)
XLA Modules:
  0.0 276.0 jit_solution(1793755062558452575)
XLA Ops:
  8.8 86.2 %all-gather.3.cloned.1.call-done = bf16[2048,1536]{1,0:T(8,128)(2,1)} async-done(((bf16[128,1536]{1,0:T(8,128)(2,1)}), bf16[2048,1536]{1,0:T(8,128)(2,1)}) %all-gather.3.cloned.1.call-update) | async-done | bytes 6291472 | tf_op jit(solution)/shard_map/all_gather | solution.py:39
  98.7 3.6 %collective-permute-start = (bf16[160,2,256]{2,0,1:T(8,128)(2,1)S(1)}, bf16[160,2,256]{2,0,1:T(8,128)(2,1)S(1)}, u32[]{:S(2)}, u32[]{:S(2)}) collective-permute-start(bf16[160,2,256]{2,0,1:T(8,128)(2,1)S(1)} %pad_maximum_fusion.1), channel_id=1, source_target_pairs={{0,16},{16,32},{32,48},{48,64},{64,80},{80,96},{96,112},{112,128},... | collective-permute-start | bytes 491528 | tf_op jit(solution)/shard_map/ppermute | solution.py:25
  102.3 5.5 %collective-permute-start.1 = (bf16[160,2,256]{2,0,1:T(8,128)(2,1)S(1)}, bf16[160,2,256]{2,0,1:T(8,128)(2,1)S(1)}, u32[]{:S(2)}, u32[]{:S(2)}) collective-permute-start(bf16[160,2,256]{2,0,1:T(8,128)(2,1)S(1)} %pad_maximum_fusion.1), channel_id=1, source_target_pairs={{0,240},{16,0},{32,16},{48,32},{64,48},{80,64},{96,80},{112,96},{1... | collective-permute-start | bytes 491528 | tf_op jit(solution)/shard_map/ppermute | solution.py:28
  107.7 2.6 collective-permute-done
  113.0 5.2 %collective-permute-start.3 = (bf16[160,2,256]{2,0,1:T(8,128)(2,1)S(1)}, bf16[160,2,256]{2,0,1:T(8,128)(2,1)S(1)}, u32[]{:S(2)}, u32[]{:S(2)}) collective-permute-start(bf16[160,2,256]{2,0,1:T(8,128)(2,1)S(1)} %collective-permute-done.1), channel_id=1, source_target_pairs={{0,240},{16,0},{32,16},{48,32},{64,48},{80,64},{96,80},{112,96},{1... | collective-permute-start | bytes 491528 | tf_op jit(solution)/shard_map/ppermute | solution.py:28
  121.2 5.5 %collective-permute-start.5 = (bf16[160,2,256]{2,0,1:T(8,128)(2,1)S(1)}, bf16[160,2,256]{2,0,1:T(8,128)(2,1)S(1)}, u32[]{:S(2)}, u32[]{:S(2)}) collective-permute-start(bf16[160,2,256]{2,0,1:T(8,128)(2,1)S(1)} %collective-permute-done.3), channel_id=1, source_target_pairs={{0,240},{16,0},{32,16},{48,32},{64,48},{80,64},{96,80},{112,96},{1... | collective-permute-start | bytes 491528 | tf_op jit(solution)/shard_map/ppermute | solution.py:28
  130.2 5.2 %collective-permute-start.7 = (bf16[160,2,256]{2,0,1:T(8,128)(2,1)S(1)}, bf16[160,2,256]{2,0,1:T(8,128)(2,1)S(1)}, u32[]{:S(2)}, u32[]{:S(2)}) collective-permute-start(bf16[160,2,256]{2,0,1:T(8,128)(2,1)S(1)} %collective-permute-done.5), channel_id=1, source_target_pairs={{0,240},{16,0},{32,16},{48,32},{64,48},{80,64},{96,80},{112,96},{1... | collective-permute-start | bytes 491528 | tf_op jit(solution)/shard_map/ppermute | solution.py:28
  138.1 3.0 %fusion.20 = f32[160,1024]{1,0:T(8,128)S(1)} fusion(bf16[2048,1536]{1,0:T(8,128)(2,1)} %all-gather.3.cloned.1.call-done, bf16[1,160,2048]{2,1,0:T(8,128)(2,1)S(1)} %copy-done), kind=kOutput, calls=%fused_computation.27 | convolution fusion | flops 671088640 | bytes 5505024 | tf_op jit(solution)/shard_map/dot_general | solution.py:84
  141.9 5.2 %collective-permute-start.9 = (bf16[160,2,256]{2,0,1:T(8,128)(2,1)S(1)}, bf16[160,2,256]{2,0,1:T(8,128)(2,1)S(1)}, u32[]{:S(2)}, u32[]{:S(2)}) collective-permute-start(bf16[160,2,256]{2,0,1:T(8,128)(2,1)S(1)} %collective-permute-done.7), channel_id=1, source_target_pairs={{0,240},{16,0},{32,16},{48,32},{64,48},{80,64},{96,80},{112,96},{1... | collective-permute-start | bytes 491528 | tf_op jit(solution)/shard_map/ppermute | solution.py:28
  149.9 5.6 %collective-permute-start.11 = (bf16[160,2,256]{2,0,1:T(8,128)(2,1)S(1)}, bf16[160,2,256]{2,0,1:T(8,128)(2,1)}, u32[]{:S(2)}, u32[]{:S(2)}) collective-permute-start(bf16[160,2,256]{2,0,1:T(8,128)(2,1)S(1)} %collective-permute-done.9), channel_id=1, source_target_pairs={{0,240},{16,0},{32,16},{48,32},{64,48},{80,64},{96,80},{112,96},{1... | collective-permute-start | bytes 491528 | tf_op jit(solution)/shard_map/ppermute | solution.py:28
  158.4 5.8 %collective-permute-start.13 = (bf16[160,2,256]{2,0,1:T(8,128)(2,1)}, bf16[160,2,256]{2,0,1:T(8,128)(2,1)}, u32[]{:S(2)}, u32[]{:S(2)}) collective-permute-start(bf16[160,2,256]{2,0,1:T(8,128)(2,1)} %collective-permute-done.11), channel_id=1, source_target_pairs={{0,240},{16,0},{32,16},{48,32},{64,48},{80,64},{96,80},{112,96},{1... | collective-permute-start | bytes 491528 | tf_op jit(solution)/shard_map/ppermute | solution.py:28
  170.1 3.7 %dynamic_update_slice.52 = bf16[2560,2,256]{0,2,1:T(8,128)(2,1)S(1)} dynamic-update-slice(bf16[2560,2,256]{0,2,1:T(8,128)(2,1)S(1)} %broadcast_in_dim.12, bf16[160,2,256]{0,2,1:T(8,128)(2,1)} %copy.28, s32[]{:T(128)S(6)} %select_n.132, s32[]{:T(128)} %copy.72, s32[]{:T(128)} %copy.72) | dynamic-update-slice | bytes 327684 | tf_op jit(solution)/shard_map/dynamic_update_slice | solution.py:21
  180.0 3.2 %dynamic_update_slice.54 = bf16[2560,2,256]{0,2,1:T(8,128)(2,1)S(1)} dynamic-update-slice(bf16[2560,2,256]{0,2,1:T(8,128)(2,1)S(1)} %dynamic_update_slice.53, bf16[160,2,256]{0,2,1:T(8,128)(2,1)S(1)} %copy.30, s32[]{:T(128)S(6)} %select_n.136, s32[]{:T(128)} %copy.72, s32[]{:T(128)} %copy.72) | dynamic-update-slice | bytes 327684 | tf_op jit(solution)/shard_map/dynamic_update_slice | solution.py:29
  184.2 2.3 dynamic_update_slice.55
  187.6 3.2 %dynamic_update_slice.56 = bf16[2560,2,256]{0,2,1:T(8,128)(2,1)S(1)} dynamic-update-slice(bf16[2560,2,256]{0,2,1:T(8,128)(2,1)S(1)} %dynamic_update_slice.55, bf16[160,2,256]{0,2,1:T(8,128)(2,1)S(1)} %copy.32, s32[]{:T(128)S(6)} %select_n.140, s32[]{:T(128)} %copy.72, s32[]{:T(128)} %copy.72) | dynamic-update-slice | bytes 327684 | tf_op jit(solution)/shard_map/dynamic_update_slice | solution.py:29
  191.8 3.2 %dynamic_update_slice.57 = bf16[2560,2,256]{0,2,1:T(8,128)(2,1)S(1)} dynamic-update-slice(bf16[2560,2,256]{0,2,1:T(8,128)(2,1)S(1)} %dynamic_update_slice.56, bf16[160,2,256]{0,2,1:T(8,128)(2,1)S(1)} %copy.33, s32[]{:T(128)S(6)} %select_n.142, s32[]{:T(128)} %copy.72, s32[]{:T(128)} %copy.72) | dynamic-update-slice | bytes 327684 | tf_op jit(solution)/shard_map/dynamic_update_slice | solution.py:26
  196.1 3.2 %dynamic_update_slice.58 = bf16[2560,2,256]{0,2,1:T(8,128)(2,1)S(1)} dynamic-update-slice(bf16[2560,2,256]{0,2,1:T(8,128)(2,1)S(1)} %dynamic_update_slice.57, bf16[160,2,256]{0,2,1:T(8,128)(2,1)S(1)} %copy.34, s32[]{:T(128)S(6)} %select_n.144, s32[]{:T(128)} %copy.72, s32[]{:T(128)} %copy.72) | dynamic-update-slice | bytes 327684 | tf_op jit(solution)/shard_map/dynamic_update_slice | solution.py:29
  200.3 2.5 dynamic_update_slice.59
  203.8 2.5 dynamic_update_slice.60
  207.4 3.2 %dynamic_update_slice.61 = bf16[2560,2,256]{0,2,1:T(8,128)(2,1)S(1)} dynamic-update-slice(bf16[2560,2,256]{0,2,1:T(8,128)(2,1)S(1)} %dynamic_update_slice.60, bf16[160,2,256]{0,2,1:T(8,128)(2,1)S(1)} %copy.37, s32[]{:T(128)S(6)} %select_n.150, s32[]{:T(128)} %copy.72, s32[]{:T(128)} %copy.72) | dynamic-update-slice | bytes 327684 | tf_op jit(solution)/shard_map/dynamic_update_slice | solution.py:26
  211.6 3.2 %dynamic_update_slice.62 = bf16[2560,2,256]{0,2,1:T(8,128)(2,1)S(1)} dynamic-update-slice(bf16[2560,2,256]{0,2,1:T(8,128)(2,1)S(1)} %dynamic_update_slice.61, bf16[160,2,256]{0,2,1:T(8,128)(2,1)S(1)} %copy.38, s32[]{:T(128)S(6)} %select_n.152, s32[]{:T(128)} %copy.72, s32[]{:T(128)} %copy.72) | dynamic-update-slice | bytes 327684 | tf_op jit(solution)/shard_map/dynamic_update_slice | solution.py:29
  215.8 3.2 %dynamic_update_slice.63 = bf16[2560,2,256]{0,2,1:T(8,128)(2,1)S(1)} dynamic-update-slice(bf16[2560,2,256]{0,2,1:T(8,128)(2,1)S(1)} %dynamic_update_slice.62, bf16[160,2,256]{0,2,1:T(8,128)(2,1)S(1)} %copy.39, s32[]{:T(128)S(6)} %select_n.154, s32[]{:T(128)} %copy.72, s32[]{:T(128)} %copy.72) | dynamic-update-slice | bytes 327684 | tf_op jit(solution)/shard_map/dynamic_update_slice | solution.py:26
  220.0 3.2 %dynamic_update_slice.64 = bf16[2560,2,256]{0,2,1:T(8,128)(2,1)S(1)} dynamic-update-slice(bf16[2560,2,256]{0,2,1:T(8,128)(2,1)S(1)} %dynamic_update_slice.63, bf16[160,2,256]{0,2,1:T(8,128)(2,1)S(1)} %copy.40, s32[]{:T(128)S(6)} %select_n.156, s32[]{:T(128)} %copy.72, s32[]{:T(128)} %copy.72) | dynamic-update-slice | bytes 327684 | tf_op jit(solution)/shard_map/dynamic_update_slice | solution.py:29
  224.3 3.2 %dynamic_update_slice.65 = bf16[2560,2,256]{0,2,1:T(8,128)(2,1)S(1)} dynamic-update-slice(bf16[2560,2,256]{0,2,1:T(8,128)(2,1)S(1)} %dynamic_update_slice.64, bf16[160,2,256]{0,2,1:T(8,128)(2,1)S(1)} %copy.41, s32[]{:T(128)S(6)} %select_n.158, s32[]{:T(128)} %copy.72, s32[]{:T(128)} %copy.72) | dynamic-update-slice | bytes 327684 | tf_op jit(solution)/shard_map/dynamic_update_slice | solution.py:26
  228.5 3.2 %dynamic_update_slice.66 = bf16[2560,2,256]{0,2,1:T(8,128)(2,1)S(1)} dynamic-update-slice(bf16[2560,2,256]{0,2,1:T(8,128)(2,1)S(1)} %dynamic_update_slice.65, bf16[160,2,256]{0,2,1:T(8,128)(2,1)S(1)} %copy.42, s32[]{:T(128)S(6)} %select_n.160, s32[]{:T(128)} %copy.72, s32[]{:T(128)} %copy.72) | dynamic-update-slice | bytes 327684 | tf_op jit(solution)/shard_map/dynamic_update_slice | solution.py:29
  232.7 2.5 dynamic_update_slice.67
  236.9 28.2 %while.10 = (s32[]{:T(128)}, bf16[4,160,256]{1,2,0:T(8,128)(2,1)}, bf16[4,2560,1,64]{1,3,2,0:T(8,128)(2,1)}, bf16[4,2560,1,64]{1,3,2,0:T(8,128)(2,1)}, bf16[4,160,1,4,64]{1,4,3,2,0:T(8,128)(2,1)}, /*index=5*/s32[]{:T(128)}) while((s32[]{:T(128)}, bf16[4,160,256]{1,2,0:T(8,128)(2,1)}, bf16[4,2560,1,64]{1,3,2,0:T(8,128)(2,1)}, ...), condition=%wide.region_5.6_spmd, body=%wide.region_2.5_spmd.sunk | while | flops 434215680 | bytes 20757060 | solution.py:108
  240.3 2.9 %fusion.44 = bf16[64,4,160]{2,0,1:T(8,128)(2,1)S(1)} fusion(f32[4,160]{1,0:T(4,128)S(1)} %fusion.43, f32[4,160]{1,0:T(4,128)S(1)} %get-tuple-element.91, f32[2560,160,4]{0,1,2:T(8,128)S(1)} %get-tuple-element.90, bf16[4,2560,1,64]{1,3,2,0:T(8,128)(2,1)} %get-tuple-element.106, s32[]{:T(128)} %get-tuple-element.98), kind=kOutput, calls=%fused_computation.7.clone.1 | convolution fusion | flops 216309760 | bytes 6968832 | tf_op jit(solution)/shard_map/while/body/eval_jaxpr/kgqs,skd->qkgd/dot_general | solution.py:71
  247.4 2.9 %fusion.44 = bf16[64,4,160]{2,0,1:T(8,128)(2,1)S(1)} fusion(f32[4,160]{1,0:T(4,128)S(1)} %fusion.43, f32[4,160]{1,0:T(4,128)S(1)} %get-tuple-element.91, f32[2560,160,4]{0,1,2:T(8,128)S(1)} %get-tuple-element.90, bf16[4,2560,1,64]{1,3,2,0:T(8,128)(2,1)} %get-tuple-element.106, s32[]{:T(128)} %get-tuple-element.98), kind=kOutput, calls=%fused_computation.7.clone.1 | convolution fusion | flops 216309760 | bytes 6968832 | tf_op jit(solution)/shard_map/while/body/eval_jaxpr/kgqs,skd->qkgd/dot_general | solution.py:71
  254.4 2.9 %fusion.44 = bf16[64,4,160]{2,0,1:T(8,128)(2,1)S(1)} fusion(f32[4,160]{1,0:T(4,128)S(1)} %fusion.43, f32[4,160]{1,0:T(4,128)S(1)} %get-tuple-element.91, f32[2560,160,4]{0,1,2:T(8,128)S(1)} %get-tuple-element.90, bf16[4,2560,1,64]{1,3,2,0:T(8,128)(2,1)} %get-tuple-element.106, s32[]{:T(128)} %get-tuple-element.98), kind=kOutput, calls=%fused_computation.7.clone.1 | convolution fusion | flops 216309760 | bytes 6968832 | tf_op jit(solution)/shard_map/while/body/eval_jaxpr/kgqs,skd->qkgd/dot_general | solution.py:71
  261.5 2.9 %fusion.44 = bf16[64,4,160]{2,0,1:T(8,128)(2,1)S(1)} fusion(f32[4,160]{1,0:T(4,128)S(1)} %fusion.43, f32[4,160]{1,0:T(4,128)S(1)} %get-tuple-element.91, f32[2560,160,4]{0,1,2:T(8,128)S(1)} %get-tuple-element.90, bf16[4,2560,1,64]{1,3,2,0:T(8,128)(2,1)} %get-tuple-element.106, s32[]{:T(128)} %get-tuple-element.98), kind=kOutput, calls=%fused_computation.7.clone.1 | convolution fusion | flops 216309760 | bytes 6968832 | tf_op jit(solution)/shard_map/while/body/eval_jaxpr/kgqs,skd->qkgd/dot_general | solution.py:71
  265.1 4.1 %fusion.19 = bf16[1,160,2048]{2,1,0:T(8,128)(2,1)} fusion(bf16[160,1024]{0,1:T(8,128)(2,1)} %bitcast.105, bf16[1024,2048]{1,0:T(8,128)(2,1)} %all-gather.5.cloned.1.call-done), kind=kOutput, calls=%fused_computation.22 | convolution fusion | flops 671416320 | bytes 5177344 | tf_op jit(solution)/shard_map/dot_general | solution.py:110
  (109 shorter events, 67.5 us)
Async XLA Ops:
  6.5 88.5 %copy-start = (bf16[1,160,2048]{2,1,0:T(8,128)(2,1)S(1)}, bf16[1,160,2048]{2,1,0:T(8,128)(2,1)}, u32[]{:S(2)}) copy-start(bf16[1,160,2048]{2,1,0:T(8,128)(2,1)} %param.9) | copy-start | bytes 1966084
  6.6 90.2 %copy-start.11 = (f32[64]{0:T(128)S(1)}, f32[64]{0:T(128)}, u32[]{:S(2)}) copy-start(f32[64]{0:T(128)} %param.15) | copy-start | bytes 772
  6.6 88.5 %all-gather.3.cloned.1.call-start = ((), (), s32[]{:S(2)}) async-start(), calls=%async_computation | async-start | bytes 6684672 | tf_op jit(solution)/shard_map/all_gather | solution.py:39
  8.5 256.6 %all-gather.5.cloned.1.call-start = ((), (), s32[]{:S(2)}) async-start(), calls=%async_computation.1 | async-start | bytes 4456448 | tf_op jit(solution)/shard_map/all_gather | solution.py:112
  98.7 11.7 %collective-permute-start = (bf16[160,2,256]{2,0,1:T(8,128)(2,1)S(1)}, bf16[160,2,256]{2,0,1:T(8,128)(2,1)S(1)}, u32[]{:S(2)}, u32[]{:S(2)}) collective-permute-start(bf16[160,2,256]{2,0,1:T(8,128)(2,1)S(1)} %pad_maximum_fusion.1), channel_id=1, source_target_pairs={{0,16},{16,32},{32,48},{48,64},{64,80},{80,96},{96,112},{112,128},... | collective-permute-start | bytes 491528 | tf_op jit(solution)/shard_map/ppermute | solution.py:25
  102.3 10.0 %collective-permute-start.1 = (bf16[160,2,256]{2,0,1:T(8,128)(2,1)S(1)}, bf16[160,2,256]{2,0,1:T(8,128)(2,1)S(1)}, u32[]{:S(2)}, u32[]{:S(2)}) collective-permute-start(bf16[160,2,256]{2,0,1:T(8,128)(2,1)S(1)} %pad_maximum_fusion.1), channel_id=1, source_target_pairs={{0,240},{16,0},{32,16},{48,32},{64,48},{80,64},{96,80},{112,96},{1... | collective-permute-start | bytes 491528 | tf_op jit(solution)/shard_map/ppermute | solution.py:28
  110.3 17.3 %copy-start.3 = (bf16[160,2,256]{2,0,1:T(8,128)(2,1)}, bf16[160,2,256]{2,0,1:T(8,128)(2,1)S(1)}, u32[]{:S(2)}) copy-start(bf16[160,2,256]{2,0,1:T(8,128)(2,1)S(1)} %collective-permute-done) | copy-start | bytes 491524
  110.3 8.9 %collective-permute-start.2 = (bf16[160,2,256]{2,0,1:T(8,128)(2,1)S(1)}, bf16[160,2,256]{2,0,1:T(8,128)(2,1)S(1)}, u32[]{:S(2)}, u32[]{:S(2)}) collective-permute-start(bf16[160,2,256]{2,0,1:T(8,128)(2,1)S(1)} %collective-permute-done), channel_id=1, source_target_pairs={{0,16},{16,32},{32,48},{48,64},{64,80},{80,96},{96,112},{112,128},... | collective-permute-start | bytes 491528 | tf_op jit(solution)/shard_map/ppermute | solution.py:25
  112.3 0.7 copy-start.1
  113.0 8.2 %collective-permute-start.3 = (bf16[160,2,256]{2,0,1:T(8,128)(2,1)S(1)}, bf16[160,2,256]{2,0,1:T(8,128)(2,1)S(1)}, u32[]{:S(2)}, u32[]{:S(2)}) collective-permute-start(bf16[160,2,256]{2,0,1:T(8,128)(2,1)S(1)} %collective-permute-done.1), channel_id=1, source_target_pairs={{0,240},{16,0},{32,16},{48,32},{64,48},{80,64},{96,80},{112,96},{1... | collective-permute-start | bytes 491528 | tf_op jit(solution)/shard_map/ppermute | solution.py:28
  119.2 2.0 copy-start.2
  119.2 8.4 %collective-permute-start.4 = (bf16[160,2,256]{2,0,1:T(8,128)(2,1)S(1)}, bf16[160,2,256]{2,0,1:T(8,128)(2,1)S(1)}, u32[]{:S(2)}, u32[]{:S(2)}) collective-permute-start(bf16[160,2,256]{2,0,1:T(8,128)(2,1)S(1)} %collective-permute-done.2), channel_id=1, source_target_pairs={{0,16},{16,32},{32,48},{48,64},{64,80},{80,96},{96,112},{112,128},... | collective-permute-start | bytes 491528 | tf_op jit(solution)/shard_map/ppermute | solution.py:25
  121.2 14.9 %copy-start.4 = (bf16[160,2,256]{2,0,1:T(8,128)(2,1)}, bf16[160,2,256]{2,0,1:T(8,128)(2,1)S(1)}, u32[]{:S(2)}) copy-start(bf16[160,2,256]{2,0,1:T(8,128)(2,1)S(1)} %collective-permute-done.3) | copy-start | bytes 491524
  121.2 9.0 %collective-permute-start.5 = (bf16[160,2,256]{2,0,1:T(8,128)(2,1)S(1)}, bf16[160,2,256]{2,0,1:T(8,128)(2,1)S(1)}, u32[]{:S(2)}, u32[]{:S(2)}) collective-permute-start(bf16[160,2,256]{2,0,1:T(8,128)(2,1)S(1)} %collective-permute-done.3), channel_id=1, source_target_pairs={{0,240},{16,0},{32,16},{48,32},{64,48},{80,64},{96,80},{112,96},{1... | collective-permute-start | bytes 491528 | tf_op jit(solution)/shard_map/ppermute | solution.py:28
  127.7 8.4 %copy-start.5 = (bf16[160,2,256]{2,0,1:T(8,128)(2,1)}, bf16[160,2,256]{2,0,1:T(8,128)(2,1)S(1)}, u32[]{:S(2)}) copy-start(bf16[160,2,256]{2,0,1:T(8,128)(2,1)S(1)} %collective-permute-done.4) | copy-start | bytes 491524
  127.7 8.4 %collective-permute-start.6 = (bf16[160,2,256]{2,0,1:T(8,128)(2,1)S(1)}, bf16[160,2,256]{2,0,1:T(8,128)(2,1)S(1)}, u32[]{:S(2)}, u32[]{:S(2)}) collective-permute-start(bf16[160,2,256]{2,0,1:T(8,128)(2,1)S(1)} %collective-permute-done.4), channel_id=1, source_target_pairs={{0,16},{16,32},{32,48},{48,64},{64,80},{80,96},{96,112},{112,128},... | collective-permute-start | bytes 491528 | tf_op jit(solution)/shard_map/ppermute | solution.py:25
  130.2 10.9 %copy-start.6 = (bf16[160,2,256]{2,0,1:T(8,128)(2,1)}, bf16[160,2,256]{2,0,1:T(8,128)(2,1)S(1)}, u32[]{:S(2)}) copy-start(bf16[160,2,256]{2,0,1:T(8,128)(2,1)S(1)} %collective-permute-done.5) | copy-start | bytes 491524
  130.2 11.7 %collective-permute-start.7 = (bf16[160,2,256]{2,0,1:T(8,128)(2,1)S(1)}, bf16[160,2,256]{2,0,1:T(8,128)(2,1)S(1)}, u32[]{:S(2)}, u32[]{:S(2)}) collective-permute-start(bf16[160,2,256]{2,0,1:T(8,128)(2,1)S(1)} %collective-permute-done.5), channel_id=1, source_target_pairs={{0,240},{16,0},{32,16},{48,32},{64,48},{80,64},{96,80},{112,96},{1... | collective-permute-start | bytes 491528 | tf_op jit(solution)/shard_map/ppermute | solution.py:28
  136.1 5.0 %copy-start.7 = (bf16[160,2,256]{2,0,1:T(8,128)(2,1)}, bf16[160,2,256]{2,0,1:T(8,128)(2,1)S(1)}, u32[]{:S(2)}) copy-start(bf16[160,2,256]{2,0,1:T(8,128)(2,1)S(1)} %collective-permute-done.6) | copy-start | bytes 491524
  136.1 11.0 %collective-permute-start.8 = (bf16[160,2,256]{2,0,1:T(8,128)(2,1)S(1)}, bf16[160,2,256]{2,0,1:T(8,128)(2,1)}, u32[]{:S(2)}, u32[]{:S(2)}) collective-permute-start(bf16[160,2,256]{2,0,1:T(8,128)(2,1)S(1)} %collective-permute-done.6), channel_id=1, source_target_pairs={{0,16},{16,32},{32,48},{48,64},{64,80},{80,96},{96,112},{112,128},... | collective-permute-start | bytes 491528 | tf_op jit(solution)/shard_map/ppermute | solution.py:25
  141.1 16.6 %copy-start.12 = (f32[64]{0:T(128)S(1)}, f32[64]{0:T(128)}, u32[]{:S(2)}) copy-start(f32[64]{0:T(128)} %param.14) | copy-start | bytes 772
  141.9 25.3 %copy-start.8 = (bf16[160,2,256]{2,0,1:T(8,128)(2,1)}, bf16[160,2,256]{2,0,1:T(8,128)(2,1)S(1)}, u32[]{:S(2)}) copy-start(bf16[160,2,256]{2,0,1:T(8,128)(2,1)S(1)} %collective-permute-done.7) | copy-start | bytes 491524
  141.9 8.0 %collective-permute-start.9 = (bf16[160,2,256]{2,0,1:T(8,128)(2,1)S(1)}, bf16[160,2,256]{2,0,1:T(8,128)(2,1)S(1)}, u32[]{:S(2)}, u32[]{:S(2)}) collective-permute-start(bf16[160,2,256]{2,0,1:T(8,128)(2,1)S(1)} %collective-permute-done.7), channel_id=1, source_target_pairs={{0,240},{16,0},{32,16},{48,32},{64,48},{80,64},{96,80},{112,96},{1... | collective-permute-start | bytes 491528 | tf_op jit(solution)/shard_map/ppermute | solution.py:28
  147.1 8.7 %collective-permute-start.10 = (bf16[160,2,256]{2,0,1:T(8,128)(2,1)}, bf16[160,2,256]{2,0,1:T(8,128)(2,1)S(1)}, u32[]{:S(2)}, u32[]{:S(2)}) collective-permute-start(bf16[160,2,256]{2,0,1:T(8,128)(2,1)} %collective-permute-done.8), channel_id=1, source_target_pairs={{0,16},{16,32},{32,48},{48,64},{64,80},{80,96},{96,112},{112,128},... | collective-permute-start | bytes 491528 | tf_op jit(solution)/shard_map/ppermute | solution.py:25
  149.9 17.3 %copy-start.9 = (bf16[160,2,256]{2,0,1:T(8,128)(2,1)}, bf16[160,2,256]{2,0,1:T(8,128)(2,1)S(1)}, u32[]{:S(2)}) copy-start(bf16[160,2,256]{2,0,1:T(8,128)(2,1)S(1)} %collective-permute-done.9) | copy-start | bytes 491524
  149.9 8.4 %collective-permute-start.11 = (bf16[160,2,256]{2,0,1:T(8,128)(2,1)S(1)}, bf16[160,2,256]{2,0,1:T(8,128)(2,1)}, u32[]{:S(2)}, u32[]{:S(2)}) collective-permute-start(bf16[160,2,256]{2,0,1:T(8,128)(2,1)S(1)} %collective-permute-done.9), channel_id=1, source_target_pairs={{0,240},{16,0},{32,16},{48,32},{64,48},{80,64},{96,80},{112,96},{1... | collective-permute-start | bytes 491528 | tf_op jit(solution)/shard_map/ppermute | solution.py:28
  155.8 11.5 %copy-start.10 = (bf16[160,2,256]{2,0,1:T(8,128)(2,1)}, bf16[160,2,256]{2,0,1:T(8,128)(2,1)S(1)}, u32[]{:S(2)}) copy-start(bf16[160,2,256]{2,0,1:T(8,128)(2,1)S(1)} %collective-permute-done.10) | copy-start | bytes 491524
  155.8 8.9 %collective-permute-start.12 = (bf16[160,2,256]{2,0,1:T(8,128)(2,1)S(1)}, bf16[160,2,256]{2,0,1:T(8,128)(2,1)}, u32[]{:S(2)}, u32[]{:S(2)}) collective-permute-start(bf16[160,2,256]{2,0,1:T(8,128)(2,1)S(1)} %collective-permute-done.10), channel_id=1, source_target_pairs={{0,16},{16,32},{32,48},{48,64},{64,80},{80,96},{96,112},{112,128},... | collective-permute-start | bytes 491528 | tf_op jit(solution)/shard_map/ppermute | solution.py:25
  158.4 69.1 %collective-permute-start.13 = (bf16[160,2,256]{2,0,1:T(8,128)(2,1)}, bf16[160,2,256]{2,0,1:T(8,128)(2,1)}, u32[]{:S(2)}, u32[]{:S(2)}) collective-permute-start(bf16[160,2,256]{2,0,1:T(8,128)(2,1)} %collective-permute-done.11), channel_id=1, source_target_pairs={{0,240},{16,0},{32,16},{48,32},{64,48},{80,64},{96,80},{112,96},{1... | collective-permute-start | bytes 491528 | tf_op jit(solution)/shard_map/ppermute | solution.py:28
  164.7 67.0 %collective-permute-start.14 = (bf16[160,2,256]{2,0,1:T(8,128)(2,1)}, bf16[160,2,256]{2,0,1:T(8,128)(2,1)}, u32[]{:S(2)}, u32[]{:S(2)}) collective-permute-start(bf16[160,2,256]{2,0,1:T(8,128)(2,1)} %collective-permute-done.12), channel_id=1, source_target_pairs={{0,16},{16,32},{32,48},{48,64},{64,80},{80,96},{96,112},{112,128},... | collective-permute-start | bytes 491528 | tf_op jit(solution)/shard_map/ppermute | solution.py:25
Sparse Core Ops, SparseCore 0:
  9.5 85.4 all-gather.2
  129.8 52.4 all-gather.4
